TPU v7x, 32 devices: a whole 2x2x4 slice. The times are simulated.
32 devices in a mesh: gr: 2 (over x), fs: 4 (over z), tp: 4 (over y, core).
Axes of the slice: x: 2, y: 2, z: 4, core: 2. Of those that a mesh axis runs over, the one named last changes fastest.
Arguments:
- prompt: bfloat16 [4096, 2048], P(('gr', 'fs', 'tp')), may hold values from -6 to 6
- train_gate: float32 [16, 2048, 256], P(None, ('gr', 'fs'), 'tp'), may hold values from -0.125 to 0.125
- train_up: float32 [16, 2048, 256], P(None, ('gr', 'fs'), 'tp'), may hold values from -0.125 to 0.125
- train_down: float32 [16, 256, 2048], P(None, 'tp', ('gr', 'fs')), may hold values from -0.375 to 0.375
- train_shared_gate: float32 [2048, 256], P(('gr', 'fs'), 'tp'), may hold values from -0.125 to 0.125
- train_shared_up: float32 [2048, 256], P(('gr', 'fs'), 'tp'), may hold values from -0.125 to 0.125
- train_shared_down: float32 [256, 2048], P('tp', ('gr', 'fs')), may hold values from -0.375 to 0.375
- norm_gain: float32 [2048], P(('gr', 'fs')), may hold values from 0.1 to 1.9
- expert_ids: int32 [4096, 8], P(('gr', 'fs', 'tp')), may hold values from 0 to 15, all different within a row; in each aligned block of 128 rows (0 to 127, 128 to 255, ...) at most 65 rows name the same one
- route_weight: float32 [4096, 8], P(('gr', 'fs', 'tp')), may hold values from 0.05 to 0.6
Outputs:
- serve_gate: bfloat16 [16, 2048, 256], P(('fs', 'tp'))
- serve_up: bfloat16 [16, 2048, 256], P(('fs', 'tp'))
- serve_down: bfloat16 [16, 256, 2048], P(('fs', 'tp'))
- serve_shared_gate: bfloat16 [2048, 256], P(None, 'tp')
- serve_shared_up: bfloat16 [2048, 256], P(None, 'tp')
- serve_shared_down: bfloat16 [256, 2048], P('tp')
- mixed_out: bfloat16 [4096, 2048], P(('gr', 'fs', 'tp'))
Inputs may be any that keep to these rules, and one draw needn't show every extreme that they name: `expert_ids`: each row names 8 different experts. Among the rows of one device no expert is named by more than 65 rows, and in some device's rows one expert is named by exactly 65.
All inputs are finite; a program needn't handle non-finite values.
Results may differ from a plain program's by a relative error of at most 0.012.
Values may be sent and summed in bfloat16 or wider, within the bound.
A program may use at most 128 MiB of HBM per device.

v0:
```python
import jax
import jax.numpy as jnp
from jax import lax
from jax.sharding import PartitionSpec as P

eps_norm = 1e-06


def regroup(stacked, lowered):
    stacked = lax.all_to_all(
        lax.all_to_all(stacked, "fs", split_axis=0, concat_axis=2, tiled=True),
        "tp",
        split_axis=0,
        concat_axis=3,
        tiled=True,
    )
    lowered = lax.all_to_all(
        lax.all_to_all(lowered, "fs", split_axis=0, concat_axis=2, tiled=True),
        "tp",
        split_axis=0,
        concat_axis=1,
        tiled=True,
    )
    return (stacked, lowered)


def body(
    prompt,
    train_gate,
    train_up,
    train_down,
    train_shared_gate,
    train_shared_up,
    train_shared_down,
    norm_gain,
    expert_ids,
    route_weight,
):
    gain_col = norm_gain[:, None]
    stacked = jnp.stack((train_gate * gain_col[None], train_up * gain_col[None]), axis=1).astype(
        jnp.bfloat16
    )
    lowered = train_down.astype(jnp.bfloat16)
    stacked, lowered = regroup(stacked, lowered)
    stacked, lowered = (
        lax.all_gather(stacked, "gr", axis=2, tiled=True),
        lax.all_gather(lowered, "gr", axis=2, tiled=True),
    )
    serve_gate = stacked[:, 0]
    serve_up = stacked[:, 1]
    serve_shared_gate, serve_shared_up, serve_shared_down = (
        lax.all_gather(
            (train_shared_gate * gain_col).astype(jnp.bfloat16), ("gr", "fs"), axis=0, tiled=True
        ),
        lax.all_gather(
            (train_shared_up * gain_col).astype(jnp.bfloat16), ("gr", "fs"), axis=0, tiled=True
        ),
        lax.all_gather(train_shared_down.astype(jnp.bfloat16), ("gr", "fs"), axis=1, tiled=True),
    )
    widened = prompt.astype(jnp.float32)
    normed = (
        widened * lax.rsqrt(jnp.mean(widened * widened, axis=-1, keepdims=True) + eps_norm)
    ).astype(jnp.bfloat16)
    block_rows = lax.all_gather(normed, "tp", axis=0, tiled=True)
    gate_val = jnp.dot(block_rows, serve_shared_gate, preferred_element_type=jnp.float32)
    up_val = jnp.dot(block_rows, serve_shared_up, preferred_element_type=jnp.float32)
    shared_act = (jax.nn.silu(gate_val) * up_val).astype(jnp.bfloat16)
    shared_sum = lax.psum_scatter(
        jnp.dot(shared_act, serve_shared_down, preferred_element_type=jnp.float32).astype(
            jnp.bfloat16
        ),
        "tp",
        scatter_dimension=0,
        tiled=True,
    ).astype(jnp.float32)
    row_count = prompt.shape[0]
    top_count = expert_ids.shape[1]
    model_width = prompt.shape[1]
    expert_count = lax.axis_size("fs") * lax.axis_size("tp")
    capacity = row_count * top_count // expert_count + 1
    flat_ids = expert_ids.reshape(-1)
    onehot = (flat_ids[:, None] == jnp.arange(expert_count, dtype=jnp.int32)[None, :]).astype(
        jnp.int32
    )
    earlier = jnp.cumsum(onehot, axis=0) - onehot
    places = jnp.sum(earlier * onehot, axis=1)
    slot_ids = (flat_ids * capacity + places).reshape(row_count, top_count)
    slot_range = jnp.arange(expert_count * capacity, dtype=jnp.int32)
    dispatch = jnp.any(slot_range[:, None, None] == slot_ids[None, :, :], axis=-1).astype(
        jnp.bfloat16
    )
    outgoing = jnp.dot(dispatch, normed, preferred_element_type=jnp.float32).astype(jnp.bfloat16)
    outgoing = outgoing.reshape(expert_count, capacity, model_width)
    arrived = lax.all_to_all(outgoing, ("fs", "tp"), split_axis=0, concat_axis=0, tiled=True)
    source_count, slot_count, width_here = arrived.shape
    arrived_rows = arrived.reshape(source_count * slot_count, width_here)
    gate_val = jnp.dot(arrived_rows, serve_gate[0], preferred_element_type=jnp.float32)
    up_val = jnp.dot(arrived_rows, serve_up[0], preferred_element_type=jnp.float32)
    hidden = (jax.nn.silu(gate_val) * up_val).astype(jnp.bfloat16)
    result = jnp.dot(hidden, lowered[0], preferred_element_type=jnp.float32).astype(jnp.bfloat16)
    result = result.reshape(source_count, slot_count, width_here)
    returned = lax.all_to_all(result, ("fs", "tp"), split_axis=0, concat_axis=0, tiled=True)
    picked = returned.reshape(expert_count * capacity, model_width)[slot_ids]
    routed = jnp.sum(route_weight[:, :, None] * picked.astype(jnp.float32), axis=1)
    mixed_out = (routed + shared_sum).astype(jnp.bfloat16)
    return (
        serve_gate,
        serve_up,
        lowered,
        serve_shared_gate,
        serve_shared_up,
        serve_shared_down,
        mixed_out,
    )


def solution(mesh):
    placed = (
        P(("gr", "fs", "tp"), None),
        P(None, ("gr", "fs"), "tp"),
        P(None, ("gr", "fs"), "tp"),
        P(None, "tp", ("gr", "fs")),
        P(("gr", "fs"), "tp"),
        P(("gr", "fs"), "tp"),
        P("tp", ("gr", "fs")),
        P(("gr", "fs")),
        P(("gr", "fs", "tp"), None),
        P(("gr", "fs", "tp"), None),
    )
    return jax.shard_map(
        body,
        mesh=mesh,
        in_specs=placed,
        out_specs=(
            P(("fs", "tp"), None, None),
            P(("fs", "tp"), None, None),
            P(("fs", "tp"), None, None),
            P(None, "tp"),
            P(None, "tp"),
            P("tp", None),
            P(("gr", "fs", "tp"), None),
        ),
        check_vma=False,
    )
```

profile of v0, /device:TPU:24, one launch (start us, length us, event | category | flops | bytes accessed | tf_op | source)
XLA Modules:
  0.0 465.2 jit_solution(16509403626507638138)
XLA Ops:
  8.0 2.1 convert_element_type.51
  10.1 5.2 %all-to-all-start.2 = ((bf16[16,64,256]{2,1,0:T(8,128)(2,1)}), bf16[16,64,256]{2,1,0:T(8,128)(2,1)S(1)}, u32[]{:S(2)}, u32[]{:S(2)}) async-start(bf16[16,64,256]{2,1,0:T(8,128)(2,1)} %convert_element_type.51), calls=%async_computation.2 | async-start | bytes 1048576 | tf_op jit(solution)/shard_map/all_to_all | solution.py:18
  15.3 1.8 fusion.20
  17.1 1.1 pad_maximum_fusion
  18.2 9.3 %all-to-all-done.2 = bf16[16,64,256]{2,1,0:T(8,128)(2,1)S(1)} async-done(((bf16[16,64,256]{2,1,0:T(8,128)(2,1)}), bf16[16,64,256]{2,1,0:T(8,128)(2,1)S(1)}, u32[]{:S(2)}, u32[]{:S(2)}) %all-to-all-start.2) | async-done | bytes 524320 | tf_op jit(solution)/shard_map/all_to_all | solution.py:18
  27.4 5.9 %all-to-all-start = ((bf16[16,2,256,64]{2,3,1,0:T(8,128)(2,1)}), bf16[16,2,256,64]{2,3,1,0:T(8,128)(2,1)S(1)}, u32[]{:S(2)}, u32[]{:S(2)}) async-start(bf16[16,2,256,64]{2,3,1,0:T(8,128)(2,1)} %pad_maximum_fusion), calls=%async_computation | async-start | bytes 2097152 | tf_op jit(solution)/shard_map/all_to_all | solution.py:11
  33.3 0.1 copy.66
  33.4 0.1 eq.43
  33.5 0.1 eq.39
  33.6 4.5 reduce-window.6
  38.1 0.1 slice.20
  38.2 0.1 copy.68
  38.4 0.1 copy.69
  38.4 0.1 broadcast_add_fusion
  38.6 0.1 reduce_sum.30
  38.7 0.9 copy.75
  39.6 16.6 %all-to-all-done = bf16[16,2,256,64]{2,3,1,0:T(8,128)(2,1)S(1)} async-done(((bf16[16,2,256,64]{2,3,1,0:T(8,128)(2,1)}), bf16[16,2,256,64]{2,3,1,0:T(8,128)(2,1)S(1)}, u32[]{:S(2)}, u32[]{:S(2)}) %all-to-all-start) | async-done | bytes 1048608 | tf_op jit(solution)/shard_map/all_to_all | solution.py:11
  56.2 3.5 all-to-all-start.3
  59.7 0.2 fusion.9
  59.9 3.8 fusion.1
  63.7 1.1 copy.74
  64.8 3.7 all-to-all-done.3
  68.5 3.5 all-to-all-start.1
  72.0 0.2 fusion.10
  72.2 0.0 copy-start
  72.2 3.2 convolution_convert_fusion.1
  75.4 4.4 reshape.67
  79.8 6.6 %all-to-all-done.1 = bf16[4,2,1024,64]{2,3,1,0:T(8,128)(2,1)S(1)} async-done(((bf16[4,2,1024,64]{2,3,1,0:T(8,128)(2,1)}), bf16[4,2,1024,64]{2,3,1,0:T(8,128)(2,1)S(1)}, u32[]{:S(2)}, u32[]{:S(2)}) %all-to-all-start.1) | async-done | bytes 1048608 | tf_op jit(solution)/shard_map/all_to_all | solution.py:10
  86.4 6.7 %all-to-all-start.4 = ((bf16[16,65,2048]{2,1,0:T(8,128)(2,1)}), bf16[16,65,2048]{2,1,0:T(8,128)(2,1)}, u32[]{:S(2)}, u32[]{:S(2)}) async-start(bf16[16,65,2048]{2,1,0:T(8,128)(2,1)} %reshape.67), calls=%async_computation.4 | async-start | bytes 9437184 | tf_op jit(solution)/shard_map/all_to_all | solution.py:94
  93.1 0.0 all-gather.4.cloned.1.call-start
  93.2 1.1 copy.63
  94.3 0.0 all-gather.4.cloned.1.call-update
  94.3 0.2 all-gather.6.cloned.1.call-start
  94.5 0.5 all-gather.6.cloned.1.call-update
  95.0 94.2 %all-to-all-done.4 = bf16[16,65,2048]{2,1,0:T(8,128)(2,1)} async-done(((bf16[16,65,2048]{2,1,0:T(8,128)(2,1)}), bf16[16,65,2048]{2,1,0:T(8,128)(2,1)}, u32[]{:S(2)}, u32[]{:S(2)}) %all-to-all-start.4) | async-done | bytes 4259872 | tf_op jit(solution)/shard_map/all_to_all | solution.py:94
  189.2 4.4 reshape.68
  193.7 5.0 %fusion.14 = f32[1040,256]{1,0:T(8,128)} fusion(bf16[1040,2048]{1,0:T(8,128)(2,1)} %reshape.68, bf16[1,2,2048,256]{2,3,1,0:T(8,128)(2,1)} %all-gather.4.cloned.1.call-done), kind=kOutput, calls=%fused_computation.24 | convolution fusion | flops 1090519040 | bytes 6373376 | tf_op jit(solution)/shard_map/dot_general | solution.py:97
  198.7 9.2 %convolution_convert_fusion = bf16[1040,2048]{1,0:T(8,128)(2,1)} fusion(bf16[1040,2048]{1,0:T(8,128)(2,1)} %reshape.68, f32[1040,256]{1,0:T(8,128)} %fusion.14, bf16[1,256,2048]{2,1,0:T(8,128)(2,1)} %all-gather.6.cloned.1.call-done, bf16[1,2,2048,256]{2,3,1,0:T(8,128)(2,1)S(1)} %copy-done.1), kind=kOutput, calls=%fused_computation.3 | convolution fusion | flops 2184765440 | bytes 11681792 | tf_op jit(solution)/shard_map/dot_general | solution.py:100
  207.9 4.4 reshape.69
  212.3 12.5 %all-to-all-start.5 = ((bf16[16,65,2048]{2,1,0:T(8,128)(2,1)}), bf16[16,65,2048]{2,1,0:T(8,128)(2,1)}, u32[]{:S(2)}, u32[]{:S(2)}) async-start(bf16[16,65,2048]{2,1,0:T(8,128)(2,1)} %reshape.69), calls=%async_computation.5 | async-start | bytes 9437184 | tf_op jit(solution)/shard_map/all_to_all | solution.py:102
  224.8 0.0 all-gather.8.cloned.1.call-start
  224.9 0.5 all-gather.8.cloned.1.call-update
  225.4 0.0 reduce-scatter.2.cloned.1.call-start
  225.5 126.7 %all_gather.20 = bf16[2048,64]{0,1:T(8,128)(2,1)S(1)} all-gather(bf16[256,64]{0,1:T(8,128)(2,1)S(1)} %get-tuple-element.40), channel_id=1, replica_groups=mesh['gr'=2,'fs'=4,'tp'=4] {'gr','fs'}, dimensions={0}, use_global_device_ids=true | all-gather | bytes 294912 | tf_op jit(solution)/shard_map/all_gather | solution.py:52
  352.3 31.2 %all_gather.21 = bf16[2048,64]{0,1:T(8,128)(2,1)S(1)} all-gather(bf16[256,64]{0,1:T(8,128)(2,1)S(1)} %get-tuple-element.39), channel_id=1, replica_groups=mesh['gr'=2,'fs'=4,'tp'=4] {'gr','fs'}, dimensions={0}, use_global_device_ids=true | all-gather | bytes 294912 | tf_op jit(solution)/shard_map/all_gather | solution.py:55
  383.5 31.4 %all_gather.22 = bf16[64,2048]{1,0:T(8,128)(2,1)S(1)} all-gather(bf16[64,256]{1,0:T(8,128)(2,1)S(1)} %convert_element_type.54), channel_id=1, replica_groups=mesh['gr'=2,'fs'=4,'tp'=4] {'gr','fs'}, dimensions={1}, use_global_device_ids=true | all-gather | bytes 294912 | tf_op jit(solution)/shard_map/all_gather | solution.py:58
  414.8 2.4 fusion.34
  417.2 4.5 convolution_convert_fusion.2
  421.7 0.0 reduce-scatter.2.cloned.1.call-update
  421.8 0.1 copy.71
  421.9 0.1 reshape.73
  422.0 0.1 copy.65
  422.1 1.7 slice_bitcast_fusion
  423.7 1.3 copy.72
  425.1 1.3 copy.73
  426.4 4.8 %reshape.70 = bf16[1040,2048]{1,0:T(8,128)(2,1)} reshape(bf16[16,65,2048]{2,1,0:T(8,128)(2,1)} %all-to-all-done.5) | data formatting | bytes 8519680 | tf_op jit(solution)/shard_map/reshape | solution.py:103
  431.2 11.6 %gather_fusion = bf16[1024,2048]{1,0:T(8,128)(2,1)} fusion(bf16[1040,2048]{1,0:T(8,128)(2,1)} %reshape.70, s32[1024]{0:T(1024)S(1)} %broadcast_clamp_fusion), kind=kCustom, calls=%fused_computation | custom fusion | bytes 8392704 | tf_op jit(solution)/shard_map/gather | solution.py:103
  442.8 6.6 %fusion = f32[128,2048]{1,0:T(8,128)S(1)} fusion(bf16[1024,2048]{1,0:T(8,128)(2,1)} %gather_fusion, f32[128,8]{1,0:T(8,128)S(1)} %copy.65), kind=kLoop, calls=%fused_computation.2 | loop fusion | flops 6029312 | bytes 5246976 | tf_op jit(solution)/shard_map/reduce_sum | solution.py:104
  449.3 3.4 reduce-scatter.2.cloned.1.call-done
  452.8 1.9 add_convert_fusion
  454.7 1.0 copy.82
  455.7 0.7 copy.83
  456.4 0.7 copy.84
  457.1 0.7 copy.85
  (35 shorter events, 0.2 us)
Async XLA Ops:
  10.1 23.2 %copy-start.8 = (s32[128,8]{0,1:T(8,128)S(1)}, s32[128,8]{0,1:T(8,128)}, u32[]{:S(2)}) copy-start(s32[128,8]{0,1:T(8,128)} %param.18) | copy-start | bytes 12292
  10.1 17.4 %all-to-all-start.2 = ((bf16[16,64,256]{2,1,0:T(8,128)(2,1)}), bf16[16,64,256]{2,1,0:T(8,128)(2,1)S(1)}, u32[]{:S(2)}, u32[]{:S(2)}) async-start(bf16[16,64,256]{2,1,0:T(8,128)(2,1)} %convert_element_type.51), calls=%async_computation.2 | async-start | bytes 1048576 | tf_op jit(solution)/shard_map/all_to_all | solution.py:18
  17.1 42.6 %copy-start.2 = (bf16[128,2048]{1,0:T(8,128)(2,1)S(1)}, bf16[128,2048]{1,0:T(8,128)(2,1)}, u32[]{:S(2)}) copy-start(bf16[128,2048]{1,0:T(8,128)(2,1)} %param.10) | copy-start | bytes 1572868
  27.4 28.8 %all-to-all-start = ((bf16[16,2,256,64]{2,3,1,0:T(8,128)(2,1)}), bf16[16,2,256,64]{2,3,1,0:T(8,128)(2,1)S(1)}, u32[]{:S(2)}, u32[]{:S(2)}) async-start(bf16[16,2,256,64]{2,3,1,0:T(8,128)(2,1)} %pad_maximum_fusion), calls=%async_computation | async-start | bytes 2097152 | tf_op jit(solution)/shard_map/all_to_all | solution.py:11
  56.2 12.3 %all-to-all-start.3 = ((bf16[4,64,1024]{2,1,0:T(8,128)(2,1)}), bf16[4,64,1024]{2,1,0:T(8,128)(2,1)S(1)}, u32[]{:S(2)}, u32[]{:S(2)}) async-start(bf16[4,64,1024]{2,1,0:T(8,128)(2,1)} %bitcast.28), calls=%async_computation.3 | async-start | bytes 1048576 | tf_op jit(solution)/shard_map/all_to_all | solution.py:17
  68.5 6.9 %copy-start.3 = (bf16[4,64,1024]{2,1,0:T(8,128)(2,1)}, bf16[4,64,1024]{2,1,0:T(8,128)(2,1)S(1)}, u32[]{:S(2)}) copy-start(bf16[4,64,1024]{2,1,0:T(8,128)(2,1)S(1)} %all-to-all-done.3) | copy-start | bytes 1572868
  68.5 17.9 %all-to-all-start.1 = ((bf16[4,2,1024,64]{2,3,1,0:T(8,128)(2,1)}), bf16[4,2,1024,64]{2,3,1,0:T(8,128)(2,1)S(1)}, u32[]{:S(2)}, u32[]{:S(2)}) async-start(bf16[4,2,1024,64]{2,3,1,0:T(8,128)(2,1)} %bitcast.26), calls=%async_computation.1 | async-start | bytes 2097152 | tf_op jit(solution)/shard_map/all_to_all | solution.py:10
  72.2 7.7 %copy-start = (bf16[128,2048]{1,0:T(8,128)(2,1)}, bf16[128,2048]{1,0:T(8,128)(2,1)S(1)}, u32[]{:S(2)}) copy-start(bf16[128,2048]{1,0:T(8,128)(2,1)S(1)} %fusion.10) | copy-start | bytes 1572868
  86.4 102.8 %all-to-all-start.4 = ((bf16[16,65,2048]{2,1,0:T(8,128)(2,1)}), bf16[16,65,2048]{2,1,0:T(8,128)(2,1)}, u32[]{:S(2)}, u32[]{:S(2)}) async-start(bf16[16,65,2048]{2,1,0:T(8,128)(2,1)} %reshape.67), calls=%async_computation.4 | async-start | bytes 9437184 | tf_op jit(solution)/shard_map/all_to_all | solution.py:94
  93.1 100.5 %all-gather.4.cloned.1.call-start = ((), (), s32[]{:S(2)}) async-start(), calls=%async_computation.7 | async-start | bytes 3145728 | tf_op jit(solution)/shard_map/all_gather | solution.py:46
  94.3 104.4 %all-gather.6.cloned.1.call-start = ((), (), s32[]{:S(2)}) async-start(), calls=%async_computation.8 | async-start | bytes 1572864 | tf_op jit(solution)/shard_map/all_gather | solution.py:47
  193.7 5.0 %copy-start.1 = (bf16[1,2,2048,256]{2,3,1,0:T(8,128)(2,1)S(1)}, bf16[1,2,2048,256]{2,3,1,0:T(8,128)(2,1)}, u32[]{:S(2)}) copy-start(bf16[1,2,2048,256]{2,3,1,0:T(8,128)(2,1)} %all-gather.4.cloned.1.call-done) | copy-start | bytes 6291460
  212.3 13.1 %copy-start.7 = (f32[64,256]{1,0:T(8,128)S(1)}, f32[64,256]{1,0:T(8,128)}, u32[]{:S(2)}) copy-start(f32[64,256]{1,0:T(8,128)} %param.16) | copy-start | bytes 196612
  212.3 13.1 %copy-start.5 = (f32[256,64]{0,1:T(8,128)S(1)}, f32[256,64]{0,1:T(8,128)}, u32[]{:S(2)}) copy-start(f32[256,64]{0,1:T(8,128)} %param.15) | copy-start | bytes 196612
  212.3 13.2 %copy-start.6 = (f32[256,64]{0,1:T(8,128)S(1)}, f32[256,64]{0,1:T(8,128)}, u32[]{:S(2)}) copy-start(f32[256,64]{0,1:T(8,128)} %param.14) | copy-start | bytes 196612
  212.3 13.2 %copy-start.9 = (f32[256]{0:T(256)S(1)}, f32[256]{0:T(256)}, u32[]{:S(2)}) copy-start(f32[256]{0:T(256)} %param.17) | copy-start | bytes 3076
  212.3 214.0 %all-to-all-start.5 = ((bf16[16,65,2048]{2,1,0:T(8,128)(2,1)}), bf16[16,65,2048]{2,1,0:T(8,128)(2,1)}, u32[]{:S(2)}, u32[]{:S(2)}) async-start(bf16[16,65,2048]{2,1,0:T(8,128)(2,1)} %reshape.69), calls=%async_computation.5 | async-start | bytes 9437184 | tf_op jit(solution)/shard_map/all_to_all | solution.py:102
  224.8 190.0 %all-gather.8.cloned.1.call-start = ((), (), s32[]{:S(2)}) async-start(), calls=%async_computation.9 | async-start | bytes 2621440 | tf_op jit(solution)/shard_map/all_gather | solution.py:64
  225.4 227.4 %reduce-scatter.2.cloned.1.call-start = ((), (), s32[]{:S(2)}) async-start(), calls=%async_computation.10 | async-start | bytes 2621440 | tf_op jit(solution)/shard_map/reduce_scatter | solution.py:68
  414.8 7.1 %copy-start.10 = (f32[128,8]{0,1:T(8,128)S(1)}, f32[128,8]{0,1:T(8,128)}, u32[]{:S(2)}) copy-start(f32[128,8]{0,1:T(8,128)} %param.19) | copy-start | bytes 12292
  442.8 12.0 %copy-start.4 = (bf16[1,256,2048]{2,1,0:T(8,128)(2,1)S(1)}, bf16[1,256,2048]{2,1,0:T(8,128)(2,1)}, u32[]{:S(2)}) copy-start(bf16[1,256,2048]{2,1,0:T(8,128)(2,1)} %all-gather.6.cloned.1.call-done) | copy-start | bytes 3145732
Sparse Core Ops, SparseCore 0:
  96.1 34.0 all-gather.3
  132.2 21.2 all-gather.5
Sparse Core Ops, SparseCore 1:
  227.4 44.6 all-gather.7
  421.8 30.9 reduce-scatter.1
where the time goes:
time: 468 us; the launch traced here: 465 us
  blocking collectives  189 us (40%)
  waiting for transfers between devices  135 us (29%)
  local copies, waits for them, and re-layouts  41.2 us (9%)
  starting transfers between devices  37.6 us (8%)
  matrix products  24.3 us (5%)
  other arithmetic  22.3 us (5%)
  between operations  15.7 us (3%)
    all_gather x1, blocking collectives, body(): lax.all_gather((train_shared_gate * gain_col).astype(jnp.bfloat16), ('gr'...  127 us
    all_to_all x1, waiting for transfers between devices, body(): lax.all_to_all(outgoing, ('fs', 'tp'), split_axis=0, concat_axis=0, tiled...  94.2 us
    all_gather x1, blocking collectives, body(): lax.all_gather(train_shared_down.astype(jnp.bfloat16), ('gr', 'fs'), axis...  31.4 us
    all_gather x1, blocking collectives, body(): lax.all_gather((train_shared_up * gain_col).astype(jnp.bfloat16), ('gr',...  31.2 us
    all_to_all x1, waiting for transfers between devices, regroup(): lax.all_to_all(stacked, 'fs', split_axis=0, concat_axis=2, tiled=True)  16.6 us
    all_to_all x1, starting transfers between devices, body(): lax.all_to_all(result, ('fs', 'tp'), split_axis=0, concat_axis=0, tiled=T...  12.5 us
    gather x1, local copies, waits for them, and re-layouts, body(): picked = returned.reshape(expert_count * capacity, model_width)[slot_ids]  11.6 us
  transfers between devices with their start and end apart: 10, of which 6 were waited for; matrix products, arithmetic and copies ran while one was open for 14% of the time, Pallas kernels for 0%

commit v1 on v0

--- a/solution.py
+++ b/solution.py
@@ -1,9 +1,473 @@
+import functools
+
 import jax
 import jax.numpy as jnp
 from jax import lax
+from jax.experimental import pallas as pl
+from jax.experimental.pallas import tpu as pltpu
 from jax.sharding import PartitionSpec as P
 
 eps_norm = 1e-06
+MESH = pl.DeviceIdType.MESH
+CORES = 2
+VMEM_PLAN = 40 * 2**20
+VMEM_LIMIT = 60 * 2**20
+
+
+def gather_kernel(
+    n_gr, n_fs, n_tp,
+    x_in, w_in, gu_in, dn_in, sgu_in, sdn_in,
+    x_out, w_out, gu_out, dn_out, sgu_out, sdn_out,
+    xr, wr, gr_sem, dr_sem, sgr, sdr, zs, ys, cs, as_, fs_sem, ss, loc,
+):
+    gr, z, tp = lax.axis_index("gr"), lax.axis_index("fs"), lax.axis_index("tp")
+    y, c = tp // CORES, tp % CORES
+    y_peer = (1 - y) * CORES + c
+    c_peer = y * CORES + 1 - c
+    x_peer = 1 - gr
+    rows_d = sgu_in.shape[0]
+    cols_d = sdn_in.shape[1]
+    hid = sdn_in.shape[0]
+
+    barrier = pltpu.get_barrier_semaphore()
+    for dz in range(n_fs):
+        for dt in range(n_tp):
+            if dz == 0 and dt == 0:
+                continue
+            pl.semaphore_signal(
+                barrier, inc=1, device_id_type=MESH,
+                device_id={"gr": gr, "fs": (z + dz) % n_fs, "tp": (tp + dt) % n_tp},
+            )
+    pl.semaphore_signal(
+        barrier, inc=1, device_id={"gr": x_peer, "fs": z, "tp": tp}, device_id_type=MESH
+    )
+    pl.semaphore_wait(barrier, n_fs * n_tp)
+
+    def dev(g, f, t):
+        return {"gr": g, "fs": f, "tp": t}
+
+    def remote(src, dst, send, recv, where):
+        return pltpu.make_async_remote_copy(
+            src_ref=src, dst_ref=dst, send_sem=send, recv_sem=recv,
+            device_id=where, device_id_type=MESH,
+        )
+
+    def gu_at(g, f, t):
+        return gu_out.at[t, pl.ds(pl.multiple_of((g * n_fs + f) * rows_d, 128), rows_d), :]
+
+    def dn_at(g, f, t):
+        return dn_out.at[
+            pl.ds(pl.multiple_of(t * hid, 16), hid),
+            pl.ds(pl.multiple_of((g * n_fs + f) * cols_d, 128), cols_d),
+        ]
+
+    def sgu_at(g, f):
+        return sgu_out.at[pl.ds(pl.multiple_of((g * n_fs + f) * rows_d, 128), rows_d), :]
+
+    def sdn_at(g, f):
+        return sdn_out.at[:, pl.ds(pl.multiple_of((g * n_fs + f) * cols_d, 128), cols_d)]
+
+    def block(src_own, owner, sems, slot, where):
+        xs = x_in if src_own else x_out.at[owner]
+        ws = w_in if src_own else w_out.at[owner]
+        return (
+            remote(xs, x_out.at[owner], sems.at[slot, 0], xr.at[owner], where),
+            remote(ws, w_out.at[owner], sems.at[slot, 1], wr.at[owner], where),
+        )
+
+    def shared(src_own, g, f, sems, slot, where):
+        gs = sgu_in if src_own else sgu_at(g, f)
+        ds_ = sdn_in if src_own else sdn_at(g, f)
+        k = g * n_fs + f
+        return (
+            remote(gs, sgu_at(g, f), sems.at[slot, 0], sgr.at[k], where),
+            remote(ds_, sdn_at(g, f), sems.at[slot, 1], sdr.at[k], where),
+        )
+
+    def expert(src_own, f, t, slot):
+        gs = gu_in.at[z * n_tp + tp] if src_own else gu_at(gr, f, t)
+        ds_ = dn_in.at[z * n_tp + tp] if src_own else dn_at(gr, f, t)
+        k = gr * (n_fs * n_tp) + f * n_tp + t
+        where = dev(x_peer, z, tp)
+        return (
+            remote(gs, gu_at(gr, f, t), fs_sem.at[slot, 0], gr_sem.at[k], where),
+            remote(ds_, dn_at(gr, f, t), fs_sem.at[slot, 1], dr_sem.at[k], where),
+        )
+
+    def start(copies):
+        for one in copies:
+            one.start()
+
+    own = tp * n_fs + z
+    up, down = dev(gr, z + 1, tp), dev(gr, z - 1, tp)
+    has_up, has_down = z < n_fs - 1, z > 0
+    to_y, to_c, to_x = dev(gr, z, y_peer), dev(gr, z, c_peer), dev(x_peer, z, tp)
+    pending = []
+
+    def go(cond, copies):
+        pending.append((cond, copies))
+        if cond is None:
+            start(copies)
+        else:
+            pl.when(cond)(lambda: start(copies))
+
+    go(None, expert(True, z, tp, 0))
+    go(None, shared(True, gr, z, ss, 0, to_x))
+    go(has_up, block(True, own, zs, 0, up))
+    go(has_down, block(True, own, zs, 1, down))
+    go(None, block(True, own, ys, 0, to_y))
+    go(None, block(True, own, cs, 0, to_c))
+    go(has_up, shared(True, gr, z, ss, 1, up))
+    go(has_down, shared(True, gr, z, ss, 2, down))
+    locals_ = [
+        pltpu.make_async_copy(x_in, x_out.at[own], loc.at[0]),
+        pltpu.make_async_copy(w_in, w_out.at[own], loc.at[1]),
+        pltpu.make_async_copy(gu_in.at[z * n_tp + tp], gu_at(gr, z, tp), loc.at[2]),
+        pltpu.make_async_copy(dn_in.at[z * n_tp + tp], dn_at(gr, z, tp), loc.at[3]),
+        pltpu.make_async_copy(sgu_in, sgu_at(gr, z), loc.at[4]),
+        pltpu.make_async_copy(sdn_in, sdn_at(gr, z), loc.at[5]),
+    ]
+    start(locals_)
+
+    a2a = []
+    for dz in range(n_fs):
+        for dt in range(n_tp):
+            if dz == 0 and dt == 0:
+                continue
+            f, t = (z + dz) % n_fs, (tp + dt) % n_tp
+            e, k = f * n_tp + t, dz * n_tp + dt
+            mine = gr * (n_fs * n_tp) + z * n_tp + tp
+            pair = (
+                remote(gu_in.at[e], gu_at(gr, z, tp), as_.at[k, 0], gr_sem.at[mine], dev(gr, f, t)),
+                remote(dn_in.at[e], dn_at(gr, z, tp), as_.at[k, 1], dr_sem.at[mine], dev(gr, f, t)),
+            )
+            start(pair)
+            a2a.append(pair)
+
+    def wait_expert(g, f, t):
+        k = g * (n_fs * n_tp) + f * n_tp + t
+        remote(gu_in.at[0], gu_at(g, f, t), as_.at[0, 0], gr_sem.at[k], to_x).wait_recv()
+        remote(dn_in.at[0], dn_at(g, f, t), as_.at[0, 1], dr_sem.at[k], to_x).wait_recv()
+
+    def wait_block(owner):
+        for one in block(True, owner, cs, 0, to_c):
+            one.wait_recv()
+
+    def wait_shared(g, f):
+        for one in shared(True, g, f, ss, 0, to_x):
+            one.wait_recv()
+
+    def pass_experts(dz):
+        for dt in range(n_tp):
+            if dz == 0 and dt == 0:
+                continue
+            f, t = (z + n_fs - dz) % n_fs, (tp + n_tp - dt) % n_tp
+            wait_expert(gr, f, t)
+            go(None, expert(False, f, t, dz * n_tp + dt))
+
+    pass_experts(0)
+    for d in range(1, n_fs):
+        for way in (0, 1):
+            f = z - d if way == 0 else z + d
+            there = f >= 0 if way == 0 else f < n_fs
+            more = has_up if way == 0 else has_down
+            onward = up if way == 0 else down
+            owner = tp * n_fs + f
+
+            @pl.when(there)
+            def _(f=f, owner=owner):
+                wait_block(owner)
+                wait_shared(gr, f)
+
+            slot = 2 * d + way
+            go(there & more, block(False, owner, zs, slot, onward))
+            go(there, block(False, owner, ys, slot, to_y))
+            go(there & more, shared(False, gr, f, ss, 2 * slot + 1, onward))
+            go(there, shared(False, gr, f, ss, 2 * slot, to_x))
+            go(there, block(False, owner, cs, slot, to_c))
+        pass_experts(d)
+    for k in range(n_fs):
+        f = (z + k) % n_fs
+        owner = y_peer * n_fs + f
+        wait_block(owner)
+        go(None, block(False, owner, cs, 2 * n_fs + k, to_c))
+    for f in range(n_fs):
+        for dt in range(n_tp):
+            wait_expert(x_peer, f, dt)
+        wait_shared(x_peer, f)
+        for yy in range(n_tp // CORES):
+            wait_block((yy * CORES + 1 - c) * n_fs + f)
+    for one in locals_:
+        one.wait()
+    for pair in a2a:
+        for one in pair:
+            one.wait_send()
+    for cond, copies in pending:
+        if cond is None:
+            for one in copies:
+                one.wait_send()
+        else:
+
+            @pl.when(cond)
+            def _(copies=copies):
+                for one in copies:
+                    one.wait_send()
+
+
+def reduce_kernel(
+    n_fs, n_tp,
+    x_ref, w_ref, g_ref, u_ref, dn_ref, sgu_ref, sdn_ref,
+    out_ref,
+    part, rc, ry, ru, rd, sh, cs, cr, ys, yr, us, ur, ds_, dr,
+):
+    gr, z, tp = lax.axis_index("gr"), lax.axis_index("fs"), lax.axis_index("tp")
+    y, c = tp // CORES, tp % CORES
+    has_up, has_down = z < n_fs - 1, z > 0
+    to_c = {"gr": gr, "fs": z, "tp": y * CORES + 1 - c}
+    to_y = {"gr": gr, "fs": z, "tp": (1 - y) * CORES + c}
+    up, down = {"gr": gr, "fs": z + 1, "tp": tp}, {"gr": gr, "fs": z - 1, "tp": tp}
+    rows, width = x_ref.shape[1], x_ref.shape[2]
+    half = sdn_ref.shape[0]
+
+    barrier = pltpu.get_barrier_semaphore()
+    pl.semaphore_signal(barrier, inc=1, device_id=to_c, device_id_type=MESH)
+    pl.semaphore_signal(barrier, inc=1, device_id=to_y, device_id_type=MESH)
+
+    @pl.when(has_up)
+    def _():
+        pl.semaphore_signal(barrier, inc=1, device_id=up, device_id_type=MESH)
+
+    @pl.when(has_down)
+    def _():
+        pl.semaphore_signal(barrier, inc=1, device_id=down, device_id_type=MESH)
+
+    pl.semaphore_wait(barrier, 2 + has_up.astype(jnp.int32) + has_down.astype(jnp.int32))
+
+    def remote(src, dst, send, recv, where):
+        return pltpu.make_async_remote_copy(
+            src_ref=src, dst_ref=dst, send_sem=send, recv_sem=recv,
+            device_id=where, device_id_type=MESH,
+        )
+
+    step = 2
+    chunk = min(width, 512)
+
+    def compute(group):
+        def rows_of(k, carry):
+            first = group * n_fs + k * step
+            xs = x_ref[pl.ds(first, step)].reshape(step * rows, width)
+            ws = w_ref[pl.ds(first, step)].reshape(step * rows, 1)
+            gate = jnp.dot(xs, g_ref[...], preferred_element_type=jnp.float32)
+            upv = jnp.dot(xs, u_ref[...], preferred_element_type=jnp.float32)
+            act = (jax.nn.silu(gate) * upv * ws).astype(jnp.bfloat16)
+            sh[...] = jnp.zeros_like(sh)
+
+            @pl.when(z // step == k)
+            def _():
+                both = jnp.dot(
+                    x_ref[group * n_fs + z], sgu_ref[...], preferred_element_type=jnp.float32
+                )
+                val = jax.nn.silu(both[:, :half]) * both[:, half:]
+                sh[pl.ds(pl.multiple_of((z % step) * rows, 128), rows), :] = val.astype(jnp.bfloat16)
+
+            shared = sh[...]
+
+            def cols_of(j, inner):
+                cols = pl.ds(pl.multiple_of(j * chunk, 128), chunk)
+                res = jnp.dot(act, dn_ref[:, cols], preferred_element_type=jnp.float32)
+                res = res + jnp.dot(shared, sdn_ref[:, cols], preferred_element_type=jnp.float32)
+                part[pl.ds(first, step), :, cols] = res.astype(jnp.bfloat16).reshape(
+                    step, rows, chunk
+                )
+                return inner
+
+            return lax.fori_loop(0, width // chunk, cols_of, carry)
+
+        lax.fori_loop(0, n_fs // step, rows_of, 0)
+
+    other_y, other_c = 1 - y, 1 - c
+    c_sends = []
+
+    def groups(i, carry):
+        gy = jnp.where(i % 2 == 0, other_y, y)
+        gc = jnp.where(i < 2, other_c, c)
+        group = gy * CORES + gc
+        compute(group)
+
+        @pl.when(i < 2)
+        def _():
+            remote(
+                part.at[pl.ds(group * n_fs, n_fs)], rc.at[i % 2], cs.at[i % 2], cr.at[i % 2], to_c
+            ).start()
+
+        return carry
+
+    lax.fori_loop(0, 4, groups, 0)
+
+    def c_copy(i, gy):
+        group = gy * CORES + other_c
+        return remote(part.at[pl.ds(group * n_fs, n_fs)], rc.at[i], cs.at[i], cr.at[i], to_c)
+
+    c_copy(0, other_y).wait_recv()
+    g_y = other_y * CORES + c
+    g_own = tp
+
+    def wide(v):
+        return v.astype(jnp.float32)
+
+    spots = []
+    for d in range(n_fs - 1, -1, -1):
+        for way in (0, 1):
+            if d == 0 and way == 1:
+                continue
+            t = z + d if way == 0 else z - d
+            spots.append((d, way, t, (t < n_fs) if way == 0 else (t >= 0)))
+
+    def y_copy(t):
+        return remote(part.at[g_y * n_fs + t], ry.at[t], ys.at[t], yr.at[t], to_y)
+
+    for d, way, t, there in spots:
+
+        @pl.when(there)
+        def _(t=t):
+            part[g_y * n_fs + t] = (wide(part[g_y * n_fs + t]) + wide(rc[0, t])).astype(jnp.bfloat16)
+            y_copy(t).start()
+
+    c_copy(1, y).wait_recv()
+
+    def u_copy(t):
+        return remote(part.at[g_own * n_fs + t], ru.at[t], us.at[t], ur.at[t], up)
+
+    def d_copy(t):
+        return remote(part.at[g_own * n_fs + t], rd.at[t], ds_.at[t], dr.at[t], down)
+
+    for d, way, t, there in spots:
+
+        @pl.when(there)
+        def _(d=d, way=way, t=t):
+            y_copy(t).wait_recv()
+            total = wide(part[g_own * n_fs + t]) + wide(rc[1, t]) + wide(ry[t])
+            if d == 0:
+                out_ref[...] = total.astype(jnp.bfloat16)
+
+                @pl.when(has_down & has_up)
+                def _():
+                    u_copy(t).wait_recv()
+                    d_copy(t).wait_recv()
+                    out_ref[...] = (total + wide(ru[t]) + wide(rd[t])).astype(jnp.bfloat16)
+
+                @pl.when(has_down & jnp.logical_not(has_up))
+                def _():
+                    u_copy(t).wait_recv()
+                    out_ref[...] = (total + wide(ru[t])).astype(jnp.bfloat16)
+
+                @pl.when(has_up & jnp.logical_not(has_down))
+                def _():
+                    d_copy(t).wait_recv()
+                    out_ref[...] = (total + wide(rd[t])).astype(jnp.bfloat16)
+            else:
+                copy, arrived, before = (
+                    (u_copy, ru, has_down) if way == 0 else (d_copy, rd, has_up)
+                )
+                part[g_own * n_fs + t] = total.astype(jnp.bfloat16)
+
+                @pl.when(before)
+                def _():
+                    copy(t).wait_recv()
+                    part[g_own * n_fs + t] = (total + wide(arrived[t])).astype(jnp.bfloat16)
+
+                copy(t).start()
+
+    c_copy(0, other_y).wait_send()
+    c_copy(1, y).wait_send()
+    for d, way, t, there in spots:
+
+        @pl.when(there)
+        def _(d=d, way=way, t=t):
+            y_copy(t).wait_send()
+            if d:
+                (u_copy if way == 0 else d_copy)(t).wait_send()
+
+
+def small_body(
+    n_gr, n_fs, n_tp,
+    prompt, train_gate, train_up, train_down, train_shared_gate, train_shared_up,
+    train_shared_down, norm_gain, expert_ids, route_weight,
+):
+    experts, rows_d, hid = train_gate.shape
+    cols_d = train_down.shape[2]
+    rows, width = prompt.shape
+    plane = n_fs * n_tp
+    gain_col = norm_gain[:, None]
+    gu = jnp.concatenate(
+        (train_gate * gain_col[None], train_up * gain_col[None]), axis=2
+    ).astype(jnp.bfloat16)
+    dn = train_down.astype(jnp.bfloat16)
+    sgu = jnp.concatenate(
+        (train_shared_gate * gain_col, train_shared_up * gain_col), axis=1
+    ).astype(jnp.bfloat16)
+    sdn = train_shared_down.astype(jnp.bfloat16)
+    widened = prompt.astype(jnp.float32)
+    normed = (
+        widened * lax.rsqrt(jnp.mean(widened * widened, axis=-1, keepdims=True) + eps_norm)
+    ).astype(jnp.bfloat16)
+    named = expert_ids.T[None, :, :] == jnp.arange(experts, dtype=jnp.int32)[:, None, None]
+    weights = jnp.sum(jnp.where(named, route_weight.T[None, :, :], 0.0), axis=1)
+
+    bf16 = jnp.bfloat16
+    vmem = pl.BlockSpec(memory_space=pltpu.VMEM)
+    dma = pltpu.SemaphoreType.DMA
+    full = n_gr * n_fs
+    rows_all, weights_all, gu_all, serve_down, sgu_all, serve_shared_down = pl.pallas_call(
+        functools.partial(gather_kernel, n_gr, n_fs, n_tp),
+        out_shape=(
+            jax.ShapeDtypeStruct((plane, rows, width), bf16),
+            jax.ShapeDtypeStruct((plane, experts, rows), jnp.float32),
+            jax.ShapeDtypeStruct((n_tp, full * rows_d, 2 * hid), bf16),
+            jax.ShapeDtypeStruct((n_tp * hid, full * cols_d), bf16),
+            jax.ShapeDtypeStruct((full * rows_d, 2 * hid), bf16),
+            jax.ShapeDtypeStruct((hid, full * cols_d), bf16),
+        ),
+        in_specs=[vmem] * 6,
+        out_specs=(vmem,) * 6,
+        scratch_shapes=[
+            dma((plane,)), dma((plane,)),
+            dma((n_gr * plane,)), dma((n_gr * plane,)),
+            dma((full,)), dma((full,)),
+            dma((2 * n_fs, 2)), dma((2 * n_fs, 2)), dma((3 * n_fs, 2)),
+            dma((plane, 2)), dma((plane, 2)), dma((4 * n_fs, 2)), dma((6,)),
+        ],
+        compiler_params=pltpu.CompilerParams(
+            collective_id=0, has_side_effects=True, vmem_limit_bytes=VMEM_LIMIT
+        ),
+    )(normed, weights, gu, dn, sgu, sdn)
+    serve_gate = jnp.concatenate([gu_all[t, :, :hid] for t in range(n_tp)], axis=1)
+    serve_up = jnp.concatenate([gu_all[t, :, hid:] for t in range(n_tp)], axis=1)
+    own = lax.axis_index("fs") * n_tp + lax.axis_index("tp")
+    own_weights = lax.dynamic_index_in_dim(weights_all, own, axis=1, keepdims=False)[:, :, None]
+    mixed_out = pl.pallas_call(
+        functools.partial(reduce_kernel, n_fs, n_tp),
+        out_shape=jax.ShapeDtypeStruct((rows, width), bf16),
+        in_specs=[vmem] * 7,
+        out_specs=vmem,
+        scratch_shapes=[
+            pltpu.VMEM((plane, rows, width), bf16),
+            pltpu.VMEM((2, n_fs, rows, width), bf16),
+            pltpu.VMEM((n_fs, rows, width), bf16),
+            pltpu.VMEM((n_fs, rows, width), bf16),
+            pltpu.VMEM((n_fs, rows, width), bf16),
+            pltpu.VMEM((2 * rows, hid), bf16),
+            dma((2,)), dma((2,)),
+            dma((n_fs,)), dma((n_fs,)), dma((n_fs,)), dma((n_fs,)), dma((n_fs,)), dma((n_fs,)),
+        ],
+        compiler_params=pltpu.CompilerParams(
+            collective_id=1, has_side_effects=True, vmem_limit_bytes=VMEM_LIMIT
+        ),
+    )(rows_all, own_weights, serve_gate, serve_up, serve_down, sgu_all, serve_shared_down)
+    return (
+        serve_gate[None], serve_up[None], serve_down[None],
+        sgu_all[:, :hid], sgu_all[:, hid:], serve_shared_down, mixed_out,
+    )
 
 
 def regroup(stacked, lowered):
@@ -127,8 +591,16 @@
         P(("gr", "fs", "tp"), None),
         P(("gr", "fs", "tp"), None),
     )
+    n_gr, n_fs, n_tp = (mesh.shape[name] for name in ("gr", "fs", "tp"))
+
+    def chosen(prompt, *rest):
+        held = n_fs * n_tp * prompt.size * prompt.dtype.itemsize * 5 // 2
+        if n_gr == 2 and n_tp == 2 * CORES and n_fs % 2 == 0 and held < VMEM_PLAN:
+            return small_body(n_gr, n_fs, n_tp, prompt, *rest)
+        return body(prompt, *rest)
+
     return jax.shard_map(
-        body,
+        chosen,
         mesh=mesh,
         in_specs=placed,
         out_specs=(

time: 468 us -> 205 us (0.44)
  the two profiles are of different devices: /device:TPU:24 before, /device:TPU:0 now
where the time goes in v1:
time: 205 us; the launch traced here: 204 us
  Pallas kernels  180 us (88%)
  local copies, waits for them, and re-layouts  13.7 us (7%)
  other arithmetic  10.4 us (5%)
    pallas_call x1, Pallas kernels, small_body(): pl.pallas_call(functools.partial(gather_kernel, n_gr, n_fs, n_tp), out_sh...  105 us
    pallas_call x1, Pallas kernels, small_body(): pl.pallas_call(functools.partial(reduce_kernel, n_fs, n_tp), out_shape=ja...  74.9 us
    unnamed x35, local copies, waits for them, and re-layouts  8.36 us

profile of v1, /device:TPU:0, one launch (start us, length us, event | category | flops | bytes accessed | tf_op | source)
XLA Modules:
  0.0 204.5 jit_solution(5405323672353837545)
XLA Ops:
  0.6 0.0 copy-start.4
  0.6 1.9 copy.37
  2.6 0.0 copy-done.4
  2.6 0.0 copy-start.12
  2.6 1.9 copy.39
  4.5 0.0 copy-done.12
  4.5 2.2 %multiply_convert_fusion.1 = (bf16[16,256,64]{2,1,0:T(8,128)(2,1)S(1)}, bf16[16,256,64]{2,1,0:T(8,128)(2,1)S(1)}) fusion(f32[16,256,64]{2,1,0:T(8,128)S(1)} %copy.37, f32[256]{0:T(256)S(1)} %copy-done.12, f32[16,256,64]{2,1,0:T(8,128)} %copy.39), kind=kLoop, calls=%fused_computation.1 | loop fusion | flops 1048576 | bytes 3146752 | tf_op jit(solution)/shard_map/convert.2
  6.7 0.0 copy-start.7
  6.7 0.0 copy-start.8
  6.7 0.0 copy-start.2
  6.7 0.0 copy-start.6
  6.8 1.6 pad_maximum_fusion.gu_in
  8.3 0.0 copy-done.7
  8.3 0.0 copy-start.9
  8.3 0.0 copy-start.10
  8.3 0.0 copy-start.11
  8.3 0.1 copy.41
  8.4 0.0 copy-done.8
  8.4 0.1 copy.43
  8.5 0.1 multiply_convert_fusion.3
  8.6 0.7 pad_maximum_fusion.3.sgu_in
  9.4 0.0 copy-done.2
  9.4 0.2 fusion
  9.6 1.0 fusion.1.x_in
  10.5 0.0 copy-done.6
  10.5 0.9 convert_element_type.16.dn_in
  11.4 0.0 copy-done.9
  11.4 0.6 convert_element_type.17.sdn_in
  12.0 0.0 copy-done.10
  12.0 0.0 copy-done.11
  12.0 0.6 select_reduce_fusion.w_in
  12.6 104.7 %shard_map.153 = (bf16[16,128,2048]{2,1,0:T(8,128)(2,1)}, f32[16,16,128]{2,1,0:T(8,128)}, bf16[4,2048,128]{2,1,0:T(8,128)(2,1)}, bf16[256,2048]{1,0:T(8,128)(2,1...) custom-call(bf16[128,2048]{1,0:T(8,128)(2,1)} %fusion.1.x_in, f32[16,128]{1,0:T(8,128)} %select_reduce_fusion.w_in, ...), custom_call_target="tpu_custom_call" | custom-call | tf_op jit(solution)/shard_map/pallas_call | solution.py:421
  117.3 2.9 %slice_bitcast_fusion.3 = (bf16[2048,64]{1,0:T(8,128)(2,1)S(1)}, bf16[2048,64]{1,0:T(8,128)(2,1)S(1)}, bf16[2048,64]{1,0:T(8,128)(2,1)S(1)}, bf16[2048,64]{1,0:T...) fusion(bf16[4,2048,128]{2,1,0:T(8,128)(2,1)} %get-tuple-element.13), kind=kLoop, calls=%fused_computation.12 | loop fusion | bytes 4194304 | tf_op jit(solution)/shard_map/squeeze | solution.py:445
  120.2 2.6 %pad_maximum_fusion.1 = (bf16[2048,256]{1,0:T(8,128)(2,1)}, bf16[2048,256]{1,0:T(8,128)(2,1)}) fusion(bf16[2048,64]{1,0:T(8,128)(2,1)S(1)} %get-tuple-element.51, bf16[2048,64]{1,0:T(8,128)(2,1)S(1)} %get-tuple-element.52, bf16[2048,64]{1,0:T(8,128)(2,1)S(1)} %get-tuple-element.53, bf16[2048,64]{1,0:T(8,128)(2,1)S(1)} %get-tuple-element.54, ...), kind=kLoop, calls=%fused_computation.7 | loop fusion | flops 8388608 | bytes 4194304 | tf_op jit(solution)/shard_map/concatenate | solution.py:444
  122.9 0.8 constant_dynamic-slice_fusion
  123.7 1.3 copy.45.w_ref
  125.1 0.0 copy-start
  125.1 74.9 %shard_map.154 = bf16[128,2048]{1,0:T(8,128)(2,1)} custom-call(bf16[16,128,2048]{2,1,0:T(8,128)(2,1)} %get-tuple-element.17.x_ref, f32[16,128,1]{2,1,0:T(8,128)} %copy.45.w_ref, bf16[2048,256]{1,0:T(8,128)(2,1)} %get-tuple-element.61.g_ref, bf16[2048,256]{1,0:T(8,128)(2,1)} %get-tuple-element.62.u_ref, bf16[256,2048]{1,0:T(8,128)(2,1)} %get-tuple-element.14.dn_ref, ...), custom_call_target="tpu_custom_call" | custom-call | tf_op jit(solution)/shard_map/pallas_call | solution.py:448
  199.9 0.0 copy-start.1
  199.9 0.0 copy-done
  199.9 0.2 fusion.2
  200.2 0.0 copy-start.5
  200.2 0.0 copy-start.3
  200.2 0.9 copy.46
  201.1 0.9 copy.47
  202.0 0.0 copy-done.1
  202.0 1.0 copy.51
  203.0 0.0 copy-done.5
  203.0 0.7 copy.52
  203.7 0.0 copy-done.3
  203.7 0.8 copy.53
  (1 shorter events, 0.0 us)
Async XLA Ops:
  0.6 1.9 copy-start.4
  2.6 2.0 copy-start.12
  6.7 1.6 copy-start.7
  6.7 1.7 copy-start.8
  6.7 2.6 %copy-start.2 = (bf16[128,2048]{1,0:T(8,128)(2,1)S(1)}, bf16[128,2048]{1,0:T(8,128)(2,1)}, u32[]{:S(2)}) copy-start(bf16[128,2048]{1,0:T(8,128)(2,1)} %param.10) | copy-start | bytes 1572868
  6.7 3.8 %copy-start.6 = (f32[16,64,256]{2,1,0:T(8,128)S(1)}, f32[16,64,256]{2,1,0:T(8,128)}, u32[]{:S(2)}) copy-start(f32[16,64,256]{2,1,0:T(8,128)} %param.13) | copy-start | bytes 3145732
  8.3 3.1 %copy-start.9 = (f32[64,256]{1,0:T(8,128)S(1)}, f32[64,256]{1,0:T(8,128)}, u32[]{:S(2)}) copy-start(f32[64,256]{1,0:T(8,128)} %param.16) | copy-start | bytes 196612
  8.3 3.7 %copy-start.10 = (f32[128,8]{0,1:T(8,128)S(1)}, f32[128,8]{0,1:T(8,128)}, u32[]{:S(2)}) copy-start(f32[128,8]{0,1:T(8,128)} %param.19) | copy-start | bytes 12292
  8.3 3.7 %copy-start.11 = (s32[128,8]{0,1:T(8,128)S(1)}, s32[128,8]{0,1:T(8,128)}, u32[]{:S(2)}) copy-start(s32[128,8]{0,1:T(8,128)} %param.18) | copy-start | bytes 12292
  125.1 74.9 %copy-start = (bf16[2048,128]{1,0:T(8,128)(2,1)S(1)}, bf16[2048,128]{1,0:T(8,128)(2,1)}, u32[]{:S(2)}) copy-start(bf16[2048,128]{1,0:T(8,128)(2,1)} %get-tuple-element.15.sgu_ref) | copy-start | bytes 1572868
  199.9 2.1 %copy-start.1 = (bf16[256,2048]{1,0:T(8,128)(2,1)S(1)}, bf16[256,2048]{1,0:T(8,128)(2,1)}, u32[]{:S(2)}) copy-start(bf16[256,2048]{1,0:T(8,128)(2,1)} %get-tuple-element.14.dn_ref) | copy-start | bytes 3145732
  200.2 2.8 %copy-start.5 = (bf16[64,2048]{1,0:T(8,128)(2,1)S(1)}, bf16[64,2048]{1,0:T(8,128)(2,1)}, u32[]{:S(2)}) copy-start(bf16[64,2048]{1,0:T(8,128)(2,1)} %get-tuple-element.75.sdn_ref) | copy-start | bytes 786436
  200.2 3.5 %copy-start.3 = (bf16[128,2048]{1,0:T(8,128)(2,1)S(1)}, bf16[128,2048]{1,0:T(8,128)(2,1)}, u32[]{:S(2)}) copy-start(bf16[128,2048]{1,0:T(8,128)(2,1)} %shard_map.154) | copy-start | bytes 1572868

commit v2 on v0

--- a/solution.py
+++ b/solution.py
@@ -1,9 +1,427 @@
+import functools
+
 import jax
 import jax.numpy as jnp
 from jax import lax
+from jax.experimental import pallas as pl
+from jax.experimental.pallas import tpu as pltpu
 from jax.sharding import PartitionSpec as P
 
 eps_norm = 1e-06
+MESH = pl.DeviceIdType.MESH
+CORES = 2
+VMEM_PLAN = 40 * 2**20
+VMEM_LIMIT = 60 * 2**20
+
+
+def plane_kernel(
+    n_gr, n_fs, n_tp, parts,
+    x_in, w_in, e_in, s_in,
+    gate_out, up_out, down_out, s_out, mixed_out,
+    x_all, w_all, e_all, s_gu, part, rc, ry, ru, rd, sh,
+    xr, wr, er, sr, zs, ys, cs, as_, fs_sem, ss, loc,
+    ks, kr, qs, qr, us, ur, ds_, dr,
+):
+    gr, z, tp = lax.axis_index("gr"), lax.axis_index("fs"), lax.axis_index("tp")
+    y, c = tp // CORES, tp % CORES
+    y_peer = (1 - y) * CORES + c
+    c_peer = y * CORES + 1 - c
+    x_peer = 1 - gr
+    plane = n_fs * n_tp
+    _, hid, cols_d = s_in.shape
+    sub, width = x_in.shape[1], x_in.shape[2]
+    rows = parts * sub
+
+    def dev(g, f, t):
+        return {"gr": g, "fs": f, "tp": t}
+
+    peers = [
+        (dz, dt, (z + dz) % n_fs, (tp + dt) % n_tp)
+        for dz in range(n_fs)
+        for dt in range(n_tp)
+        if dz or dt
+    ]
+    barrier = pltpu.get_barrier_semaphore()
+    for _, _, f, t in peers:
+        pl.semaphore_signal(barrier, inc=1, device_id=dev(gr, f, t), device_id_type=MESH)
+    pl.semaphore_signal(barrier, inc=1, device_id=dev(x_peer, z, tp), device_id_type=MESH)
+    pl.semaphore_wait(barrier, plane)
+
+    def remote(src, dst, send, recv, where):
+        return pltpu.make_async_remote_copy(
+            src_ref=src, dst_ref=dst, send_sem=send, recv_sem=recv,
+            device_id=where, device_id_type=MESH,
+        )
+
+    def cols_of(g, f):
+        return pl.ds(pl.multiple_of((g * n_fs + f) * cols_d, 128), cols_d)
+
+    def e_at(g, f, t):
+        return e_all.at[:, pl.ds(pl.multiple_of(t * hid, 16), hid), cols_of(g, f)]
+
+    def s_at(g, f):
+        return s_out.at[:, :, cols_of(g, f)]
+
+    def block(src_own, owner, sems, slot, where, h):
+        xs = x_in.at[h] if src_own else x_all.at[owner, h]
+        copies = [remote(xs, x_all.at[owner, h], sems.at[slot, h], xr.at[owner, h], where)]
+        if h == 0:
+            ws = w_in if src_own else w_all.at[owner]
+            copies.append(remote(ws, w_all.at[owner], sems.at[slot, parts], wr.at[owner], where))
+        return copies
+
+    def shared(src_own, g, f, slot, where):
+        src = s_in if src_own else s_at(g, f)
+        return [remote(src, s_at(g, f), ss.at[slot], sr.at[g * n_fs + f], where)]
+
+    def expert(src_own, f, t, slot):
+        src = e_in.at[z * n_tp + tp] if src_own else e_at(gr, f, t)
+        k = gr * plane + f * n_tp + t
+        return [remote(src, e_at(gr, f, t), fs_sem.at[slot], er.at[k], dev(x_peer, z, tp))]
+
+    own = tp * n_fs + z
+    up, down = dev(gr, z + 1, tp), dev(gr, z - 1, tp)
+    has_up, has_down = z < n_fs - 1, z > 0
+    to_y, to_c, to_x = dev(gr, z, y_peer), dev(gr, z, c_peer), dev(x_peer, z, tp)
+    pending = []
+
+    def start(copies):
+        for one in copies:
+            one.start()
+
+    def go(cond, copies):
+        pending.append((cond, copies))
+        if cond is None:
+            start(copies)
+        else:
+            pl.when(cond)(lambda: start(copies))
+
+    for h in range(parts):
+        go(has_up, block(True, own, zs, 0, up, h))
+        go(has_down, block(True, own, zs, 1, down, h))
+        go(None, block(True, own, ys, 0, to_y, h))
+        go(None, block(True, own, cs, 0, to_c, h))
+    go(None, expert(True, z, tp, 0))
+    go(has_up, shared(True, gr, z, 1, up))
+    go(has_down, shared(True, gr, z, 2, down))
+    go(None, shared(True, gr, z, 0, to_x))
+    locals_ = [
+        pltpu.make_async_copy(x_in, x_all.at[own], loc.at[0]),
+        pltpu.make_async_copy(w_in, w_all.at[own], loc.at[1]),
+        pltpu.make_async_copy(e_in.at[z * n_tp + tp], e_at(gr, z, tp), loc.at[2]),
+        pltpu.make_async_copy(s_in, s_at(gr, z), loc.at[3]),
+    ]
+    start(locals_)
+
+    def send_experts(want):
+        for dz, dt, f, t in peers:
+            if dz == want:
+                mine = gr * plane + z * n_tp + tp
+                go(None, [remote(
+                    e_in.at[f * n_tp + t], e_at(gr, z, tp),
+                    as_.at[dz * n_tp + dt], er.at[mine], dev(gr, f, t),
+                )])
+
+    def wait_expert(g, f, t):
+        k = g * plane + f * n_tp + t
+        remote(e_in.at[0], e_at(g, f, t), as_.at[0], er.at[k], to_x).wait_recv()
+
+    def wait_block(owner, h):
+        for one in block(True, owner, cs, 0, to_c, h):
+            one.wait_recv()
+
+    def wait_shared(g, f):
+        shared(True, g, f, 0, to_x)[0].wait_recv()
+
+    def pass_experts(want):
+        for dz, dt, _, _ in peers:
+            if dz == want:
+                f, t = (z + n_fs - dz) % n_fs, (tp + n_tp - dt) % n_tp
+                wait_expert(gr, f, t)
+                go(None, expert(False, f, t, dz * n_tp + dt))
+
+    send_experts(0)
+    send_experts(1)
+    for d in range(1, n_fs):
+        for h in range(parts):
+            for way in (0, 1):
+                f = z - d if way == 0 else z + d
+                there = f >= 0 if way == 0 else f < n_fs
+                more = has_up if way == 0 else has_down
+                onward = up if way == 0 else down
+                owner = tp * n_fs + f
+                slot = 2 * d + way
+                pl.when(there)(functools.partial(wait_block, owner, h))
+                go(there & more, block(False, owner, zs, slot, onward, h))
+                go(there, block(False, owner, ys, slot, to_y, h))
+                go(there, block(False, owner, cs, slot, to_c, h))
+                if h == parts - 1:
+                    pl.when(there)(functools.partial(wait_shared, gr, f))
+                    go(there & more, shared(False, gr, f, 2 * slot + 1, onward))
+                    go(there, shared(False, gr, f, 2 * slot, to_x))
+        if d + 1 < n_fs:
+            send_experts(d + 1)
+        pass_experts(d - 1)
+    pass_experts(n_fs - 1)
+    for k in range(n_fs):
+        f = (z + k) % n_fs
+        owner = y_peer * n_fs + f
+        for h in range(parts):
+            wait_block(owner, h)
+            go(None, block(False, owner, cs, 2 * n_fs + k, to_c, h))
+    for f in range(n_fs):
+        for t in range(n_tp):
+            wait_expert(x_peer, f, t)
+        wait_shared(x_peer, f)
+        for yy in range(n_tp // CORES):
+            for h in range(parts):
+                wait_block((yy * CORES + 1 - c) * n_fs + f, h)
+    for one in locals_:
+        one.wait()
+
+    def turn(k, carry):
+        here = pl.ds(pl.multiple_of(k * cols_d, 128), cols_d)
+        gate_out[here, :] = e_all[0, :, here].T
+        up_out[here, :] = e_all[1, :, here].T
+        s_gu[here, :] = s_out[0:2, :, here].reshape(2 * hid, cols_d).T
+        return carry
+
+    lax.fori_loop(0, n_gr * n_fs, turn, 0)
+
+    step = 2
+    chunk = min(width, 512)
+    me = z * n_tp + tp
+
+    def compute(group):
+        def rows_of(k, carry):
+            first = group * n_fs + k * step
+            xs = x_all[pl.ds(first, step)].reshape(step * rows, width)
+            ws = jnp.concatenate(
+                [
+                    jnp.broadcast_to(w_all[first + i, pl.ds(me, 1), :], (rows, rows)).T[:, :1]
+                    for i in range(step)
+                ],
+                axis=0,
+            )
+            gate = jnp.dot(xs, gate_out[...], preferred_element_type=jnp.float32)
+            upv = jnp.dot(xs, up_out[...], preferred_element_type=jnp.float32)
+            act = (jax.nn.silu(gate) * upv * ws).astype(jnp.bfloat16)
+            sh[...] = jnp.zeros_like(sh)
+
+            @pl.when(z // step == k)
+            def _():
+                both = jnp.dot(
+                    x_all[group * n_fs + z].reshape(rows, width), s_gu[...],
+                    preferred_element_type=jnp.float32,
+                )
+                val = jax.nn.silu(both[:, :hid]) * both[:, hid:]
+                sh[pl.ds(pl.multiple_of((z % step) * rows, 128), rows), :] = val.astype(jnp.bfloat16)
+
+            extra = sh[...]
+
+            def cols(j, inner):
+                at = pl.ds(pl.multiple_of(j * chunk, 128), chunk)
+                res = jnp.dot(act, e_all[2, :, at], preferred_element_type=jnp.float32)
+                res = res + jnp.dot(extra, s_out[2, :, at], preferred_element_type=jnp.float32)
+                part[pl.ds(first, step), :, :, at] = res.astype(jnp.bfloat16).reshape(
+                    step, parts, sub, chunk
+                )
+                return inner
+
+            return lax.fori_loop(0, width // chunk, cols, carry)
+
+        lax.fori_loop(0, n_fs // step, rows_of, 0)
+
+    other_y, other_c = 1 - y, 1 - c
+    g_y = y_peer
+    g_own = tp
+
+    def wide(v):
+        return v.astype(jnp.float32)
+
+    def c_copy(i):
+        group = (other_y if i == 0 else y) * CORES + other_c
+        return remote(part.at[pl.ds(group * n_fs, n_fs)], rc.at[i], ks.at[i], kr.at[i], to_c)
+
+    spots = []
+    for d in range(n_fs - 1, -1, -1):
+        for way in (0, 1):
+            if d == 0 and way == 1:
+                continue
+            t = z + d if way == 0 else z - d
+            spots.append((d, way, t, (t < n_fs) if way == 0 else (t >= 0)))
+
+    def y_copy(t, h):
+        return remote(part.at[g_y * n_fs + t, h], ry.at[t, h], qs.at[t, h], qr.at[t, h], to_y)
+
+    def u_copy(t, h):
+        return remote(part.at[g_own * n_fs + t, h], ru.at[t, h], us.at[t, h], ur.at[t, h], up)
+
+    def d_copy(t, h):
+        return remote(part.at[g_own * n_fs + t, h], rd.at[t, h], ds_.at[t, h], dr.at[t, h], down)
+
+    def phase(i, carry):
+        gy = jnp.where(i == 0, other_y, y)
+
+        def one(k, inner):
+            compute(gy * CORES + jnp.where(k == 0, other_c, c))
+
+            @pl.when(k == 0)
+            def _():
+                pl.when(i == 0)(lambda: c_copy(0).start())
+                pl.when(i == 1)(lambda: c_copy(1).start())
+
+            return inner
+
+        lax.fori_loop(0, 2, one, 0)
+
+        @pl.when(i == 0)
+        def _():
+            c_copy(0).wait_recv()
+            for _d, _way, t, there in spots:
+
+                @pl.when(there)
+                def _(t=t):
+                    for h in range(parts):
+                        at = g_y * n_fs + t
+                        part[at, h] = (wide(part[at, h]) + wide(rc[0, t, h])).astype(jnp.bfloat16)
+                        y_copy(t, h).start()
+
+        return carry
+
+    lax.fori_loop(0, 2, phase, 0)
+    c_copy(1).wait_recv()
+
+    for d, way, t, there in spots:
+
+        @pl.when(there)
+        def _(d=d, way=way, t=t):
+            at = g_own * n_fs + t
+            for h in range(parts):
+                y_copy(t, h).wait_recv()
+                total = wide(part[at, h]) + wide(rc[1, t, h]) + wide(ry[t, h])
+                if d == 0:
+                    mixed_out[h] = total.astype(jnp.bfloat16)
+
+                    @pl.when(has_down & has_up)
+                    def _():
+                        u_copy(t, h).wait_recv()
+                        d_copy(t, h).wait_recv()
+                        mixed_out[h] = (total + wide(ru[t, h]) + wide(rd[t, h])).astype(jnp.bfloat16)
+
+                    @pl.when(has_down & jnp.logical_not(has_up))
+                    def _():
+                        u_copy(t, h).wait_recv()
+                        mixed_out[h] = (total + wide(ru[t, h])).astype(jnp.bfloat16)
+
+                    @pl.when(has_up & jnp.logical_not(has_down))
+                    def _():
+                        d_copy(t, h).wait_recv()
+                        mixed_out[h] = (total + wide(rd[t, h])).astype(jnp.bfloat16)
+                else:
+                    copy, arrived, before = (
+                        (u_copy, ru, has_down) if way == 0 else (d_copy, rd, has_up)
+                    )
+                    part[at, h] = total.astype(jnp.bfloat16)
+
+                    @pl.when(before)
+                    def _():
+                        copy(t, h).wait_recv()
+                        part[at, h] = (total + wide(arrived[t, h])).astype(jnp.bfloat16)
+
+                    copy(t, h).start()
+
+    down_out[...] = e_all[2]
+    for cond, copies in pending:
+        if cond is None:
+            for one in copies:
+                one.wait_send()
+        else:
+
+            @pl.when(cond)
+            def _(copies=copies):
+                for one in copies:
+                    one.wait_send()
+    c_copy(0).wait_send()
+    c_copy(1).wait_send()
+    for d, way, t, there in spots:
+
+        @pl.when(there)
+        def _(d=d, way=way, t=t):
+            for h in range(parts):
+                y_copy(t, h).wait_send()
+                if d:
+                    (u_copy if way == 0 else d_copy)(t, h).wait_send()
+
+
+def small_body(
+    n_gr, n_fs, n_tp,
+    prompt, train_gate, train_up, train_down, train_shared_gate, train_shared_up,
+    train_shared_down, norm_gain, expert_ids, route_weight,
+):
+    experts, rows_d, hid = train_gate.shape
+    rows, width = prompt.shape
+    plane, full, parts = n_fs * n_tp, n_gr * n_fs, 2
+    sub = rows // parts
+    bf16 = jnp.bfloat16
+    e_in = jnp.stack(
+        (
+            train_gate.transpose(0, 2, 1) * norm_gain,
+            train_up.transpose(0, 2, 1) * norm_gain,
+            train_down,
+        ),
+        axis=1,
+    ).astype(bf16)
+    s_in = jnp.stack(
+        (train_shared_gate.T * norm_gain, train_shared_up.T * norm_gain, train_shared_down)
+    ).astype(bf16)
+    widened = prompt.astype(jnp.float32)
+    normed = (
+        widened * lax.rsqrt(jnp.mean(widened * widened, axis=-1, keepdims=True) + eps_norm)
+    ).astype(bf16)
+    named = expert_ids.T[None, :, :] == jnp.arange(experts, dtype=jnp.int32)[:, None, None]
+    weights = jnp.sum(jnp.where(named, route_weight.T[None, :, :], 0.0), axis=1)
+
+    vmem = pl.BlockSpec(memory_space=pltpu.VMEM)
+    dma = pltpu.SemaphoreType.DMA
+    shape = jax.ShapeDtypeStruct
+    serve_gate, serve_up, serve_down, s_all, mixed_out = pl.pallas_call(
+        functools.partial(plane_kernel, n_gr, n_fs, n_tp, parts),
+        out_shape=(
+            shape((width, n_tp * hid), bf16),
+            shape((width, n_tp * hid), bf16),
+            shape((n_tp * hid, width), bf16),
+            shape((3, hid, width), bf16),
+            shape((parts, sub, width), bf16),
+        ),
+        in_specs=[vmem] * 4,
+        out_specs=(vmem,) * 5,
+        scratch_shapes=[
+            pltpu.VMEM((plane, parts, sub, width), bf16),
+            pltpu.VMEM((plane, experts, rows), jnp.float32),
+            pltpu.VMEM((3, n_tp * hid, width), bf16),
+            pltpu.VMEM((width, 2 * hid), bf16),
+            pltpu.VMEM((plane, parts, sub, width), bf16),
+            pltpu.VMEM((2, n_fs, parts, sub, width), bf16),
+            pltpu.VMEM((n_fs, parts, sub, width), bf16),
+            pltpu.VMEM((n_fs, parts, sub, width), bf16),
+            pltpu.VMEM((n_fs, parts, sub, width), bf16),
+            pltpu.VMEM((2 * rows, hid), bf16),
+            dma((plane, parts)), dma((plane,)), dma((n_gr * plane,)), dma((full,)),
+            dma((2 * n_fs, parts + 1)), dma((2 * n_fs, parts + 1)), dma((3 * n_fs, parts + 1)),
+            dma((plane,)), dma((plane,)), dma((4 * n_fs,)), dma((4,)),
+            dma((2,)), dma((2,)),
+            dma((n_fs, parts)), dma((n_fs, parts)), dma((n_fs, parts)),
+            dma((n_fs, parts)), dma((n_fs, parts)), dma((n_fs, parts)),
+        ],
+        compiler_params=pltpu.CompilerParams(
+            collective_id=0, has_side_effects=True, vmem_limit_bytes=VMEM_LIMIT
+        ),
+    )(normed.reshape(parts, sub, width), weights, e_in, s_in)
+    return (
+        serve_gate[None], serve_up[None], serve_down[None],
+        s_all[0].T, s_all[1].T, s_all[2], mixed_out.reshape(rows, width),
+    )
 
 
 def regroup(stacked, lowered):
@@ -127,8 +545,16 @@
         P(("gr", "fs", "tp"), None),
         P(("gr", "fs", "tp"), None),
     )
+    n_gr, n_fs, n_tp = (mesh.shape[name] for name in ("gr", "fs", "tp"))
+
+    def chosen(prompt, *rest):
+        held = n_fs * n_tp * prompt.size * prompt.dtype.itemsize * 5 // 2
+        if n_gr == 2 and n_tp == 2 * CORES and n_fs % 2 == 0 and held < VMEM_PLAN:
+            return small_body(n_gr, n_fs, n_tp, prompt, *rest)
+        return body(prompt, *rest)
+
     return jax.shard_map(
-        body,
+        chosen,
         mesh=mesh,
         in_specs=placed,
         out_specs=(

time: 468 us -> 172 us (0.37)
  blocking collectives: 189 us -> 0 us
  Pallas kernels: 0 us -> 155 us
  waiting for transfers between devices: 135 us -> 0 us
  starting transfers between devices: 37.6 us -> 0 us
  local copies, waits for them, and re-layouts: 41.2 us -> 6.94 us
  matrix products: 24.3 us -> 0 us
  between operations: 15.7 us -> 0.74 us
  other arithmetic: 22.3 us -> 8.78 us
    all_gather x3 -> x0, blocking collectives: 189 us -> none  [the longest x1 127 us: body(): lax.all_gather((train_shared_gate * gain_col).astype(jnp.bfloat16), ('gr'...]
    pallas_call x0 -> x1, Pallas kernels: none -> 155 us  [small_body(): pl.pallas_call(functools.partial(plane_kernel, n_gr, n_fs, n_tp, parts),...]
    all_to_all x6 -> x0, waiting for transfers between devices: 130 us -> none  [the longest x1 94.2 us: body(): lax.all_to_all(outgoing, ('fs', 'tp'), split_axis=0, concat_axis=0, tiled...]
    all_to_all x6 -> x0, starting transfers between devices: 37.3 us -> none  [the longest x1 12.5 us: body(): lax.all_to_all(result, ('fs', 'tp'), split_axis=0, concat_axis=0, tiled=T...]
    dot_general x5 -> x0, matrix products: 24.3 us -> none  [the longest x1 9.23 us: body(): jnp.dot(hidden, lowered[0], preferred_element_type=jnp.float32)]
    reshape x4 -> x0, local copies, waits for them, and re-layouts: 18.1 us -> none  [the longest x1 4.82 us: body(): picked = returned.reshape(expert_count * capacity, model_width)[slot_ids]]
    gather x1 -> x0, local copies, waits for them, and re-layouts: 11.6 us -> none  [body(): picked = returned.reshape(expert_count * capacity, model_width)[slot_ids]]
  transfers between devices with their start and end apart: 10 -> 0, of which waited for: 6 -> 0; matrix products, arithmetic and copies ran while one was open for 14% -> 0% of each run, Pallas kernels for 0% -> 0%
where the time goes in v2:
time: 172 us
  Pallas kernels  155 us (90%)
  other arithmetic  8.78 us (5%)
  local copies, waits for them, and re-layouts  6.94 us (4%)
    pallas_call x1, Pallas kernels, small_body(): pl.pallas_call(functools.partial(plane_kernel, n_gr, n_fs, n_tp, parts),...  155 us
    unnamed x20, local copies, waits for them, and re-layouts  4.79 us

profile of v2, /device:TPU:24, one launch (start us, length us, event | category | flops | bytes accessed | tf_op | source)
XLA Modules:
  0.0 171.7 jit_solution(18120174861370031925)
XLA Ops:
  0.6 0.0 copy-start
  0.6 1.3 fusion
  2.0 0.0 copy-start.1
  2.0 0.0 copy-start.2
  2.0 0.0 copy-start.7
  2.0 1.5 select_reduce_fusion.w_in
  3.5 0.8 convert_bitcast_fusion.1
  4.3 0.9 fusion.4
  5.2 0.7 pad_maximum_fusion.1.s_in
  5.9 2.0 %fusion.1 = bf16[128,2048]{1,0:T(8,128)(2,1)} fusion(bf16[128,2048]{1,0:T(8,128)(2,1)} %param.10, f32[128]{0:T(128)S(1)} %add_rsqrt_fusion), kind=kLoop, calls=%fused_computation.4 | loop fusion | flops 786432 | bytes 1049088 | tf_op jit(solution)/shard_map/convert_element_type | solution.py:381
  7.9 0.0 copy-done
  7.9 0.1 convert_bitcast_fusion
  7.9 0.0 copy-done.1
  7.9 0.0 copy-done.2
  7.9 0.0 copy-done.7
  8.0 0.2 fusion.2
  8.2 1.3 pad_maximum_fusion.e_in
  9.5 155.2 %shard_map.153 = (bf16[2048,256]{1,0:T(8,128)(2,1)}, bf16[2048,256]{1,0:T(8,128)(2,1)}, bf16[256,2048]{1,0:T(8,128)(2,1)}, bf16[3,64,2048]{2,1,0:T(8,128)(2,1)}, bf16[2,64,2048]{2,1,0:T(8,128)(2,1)}) custom-call(bf16[2,64,2048]{2,1,0:T(8,128)(2,1)} %bitcast.39, f32[16,128]{1,0:T(8,128)} %select_reduce_fusion.w_in, ...), custom_call_target="tpu_custom_call" | custom-call | tf_op jit(solution)/shard_map/pallas_call | solution.py:388
  164.7 0.0 copy-start.5
  164.7 0.0 copy-start.4
  164.7 2.1 %slice_bitcast_fusion = (bf16[64,2048]{1,0:T(8,128)(2,1)}, bf16[2048,64]{0,1:T(8,128)(2,1)}, bf16[2048,64]{0,1:T(8,128)(2,1)}) fusion(bf16[3,64,2048]{2,1,0:T(8,128)(2,1)} %get-tuple-element.15), kind=kLoop, calls=%fused_computation.10 | loop fusion | bytes 1572864 | tf_op jit(solution)/shard_map/squeeze | solution.py:423
  166.9 0.0 copy-done.5
  166.9 1.0 copy.23
  167.9 0.0 copy-done.4
  167.9 0.0 copy-start.3
  167.9 1.0 copy.24
  168.8 0.6 copy-done.3
  169.5 0.0 copy-start.6
  169.5 1.0 copy.25
  170.4 0.4 copy-done.6
  170.9 0.8 copy.26
  (1 shorter events, 0.0 us)
Async XLA Ops:
  0.6 7.2 %copy-start = (f32[16,64,256]{2,1,0:T(8,128)S(1)}, f32[16,64,256]{2,1,0:T(8,128)}, u32[]{:S(2)}) copy-start(f32[16,64,256]{2,1,0:T(8,128)} %param.13) | copy-start | bytes 3145732
  2.0 6.0 %copy-start.1 = (f32[16,256,64]{1,2,0:T(8,128)S(1)}, f32[16,256,64]{1,2,0:T(8,128)}, u32[]{:S(2)}) copy-start(f32[16,256,64]{1,2,0:T(8,128)} %param.11) | copy-start | bytes 3145732
  2.0 6.0 %copy-start.2 = (f32[16,256,64]{1,2,0:T(8,128)S(1)}, f32[16,256,64]{1,2,0:T(8,128)}, u32[]{:S(2)}) copy-start(f32[16,256,64]{1,2,0:T(8,128)} %param.12) | copy-start | bytes 3145732
  2.0 6.0 %copy-start.7 = (f32[256]{0:T(256)S(1)}, f32[256]{0:T(256)}, u32[]{:S(2)}) copy-start(f32[256]{0:T(256)} %param.17) | copy-start | bytes 3076
  164.7 2.2 %copy-start.5 = (bf16[2048,256]{1,0:T(8,128)(2,1)S(1)}, bf16[2048,256]{1,0:T(8,128)(2,1)}, u32[]{:S(2)}) copy-start(bf16[2048,256]{1,0:T(8,128)(2,1)} %get-tuple-element.12) | copy-start | bytes 3145732
  164.7 3.1 %copy-start.4 = (bf16[2048,256]{1,0:T(8,128)(2,1)S(1)}, bf16[2048,256]{1,0:T(8,128)(2,1)}, u32[]{:S(2)}) copy-start(bf16[2048,256]{1,0:T(8,128)(2,1)} %get-tuple-element.13) | copy-start | bytes 3145732
  167.9 1.6 copy-start.3
  169.5 1.4 copy-start.6

commit v3 on v2

--- a/solution.py
+++ b/solution.py
@@ -16,11 +16,12 @@
 
 def plane_kernel(
     n_gr, n_fs, n_tp, parts,
-    x_in, w_in, e_in, s_in,
-    gate_out, up_out, down_out, s_out, mixed_out,
+    p_ref, gt_ref, ut_ref, dn_ref, sg_ref, su_ref, sd_ref, gain_ref, ids_ref, rw_ref,
+    gate_hbm, up_hbm, down_hbm, sg_hbm, su_hbm, sd_hbm, mixed_out,
+    x_in, w_in, e_in, s_in, gate_out, up_out, down_out, s_out,
     x_all, w_all, e_all, s_gu, part, rc, ry, ru, rd, sh,
     xr, wr, er, sr, zs, ys, cs, as_, fs_sem, ss, loc,
-    ks, kr, qs, qr, us, ur, ds_, dr,
+    ks, kr, qs, qr, us, ur, ds_, dr, res_sem,
 ):
     gr, z, tp = lax.axis_index("gr"), lax.axis_index("fs"), lax.axis_index("tp")
     y, c = tp // CORES, tp % CORES
@@ -45,6 +46,28 @@
     for _, _, f, t in peers:
         pl.semaphore_signal(barrier, inc=1, device_id=dev(gr, f, t), device_id_type=MESH)
     pl.semaphore_signal(barrier, inc=1, device_id=dev(x_peer, z, tp), device_id_type=MESH)
+
+    gain = gain_ref[...]
+
+    def cast(i, carry):
+        e_in[i, 0] = (gt_ref[i] * gain).astype(jnp.bfloat16)
+        e_in[i, 1] = (ut_ref[i] * gain).astype(jnp.bfloat16)
+        e_in[i, 2] = dn_ref[i].astype(jnp.bfloat16)
+        return carry
+
+    s_in[0] = (sg_ref[...] * gain).astype(jnp.bfloat16)
+    s_in[1] = (su_ref[...] * gain).astype(jnp.bfloat16)
+    s_in[2] = sd_ref[...].astype(jnp.bfloat16)
+    for h in range(parts):
+        v = p_ref[h * sub : (h + 1) * sub, :].astype(jnp.float32)
+        mean = jnp.mean(v * v, axis=-1, keepdims=True)
+        x_in[h] = (v * lax.rsqrt(mean + eps_norm)).astype(jnp.bfloat16)
+    table = jnp.zeros(w_in.shape, jnp.float32)
+    which = lax.broadcasted_iota(jnp.int32, w_in.shape, 0)
+    for k in range(ids_ref.shape[0]):
+        table = table + jnp.where(ids_ref[k : k + 1, :] == which, rw_ref[k : k + 1, :], 0.0)
+    w_in[...] = table
+    lax.fori_loop(0, plane, cast, 0)
     pl.semaphore_wait(barrier, plane)
 
     def remote(src, dst, send, recv, where):
@@ -57,7 +80,7 @@
         return pl.ds(pl.multiple_of((g * n_fs + f) * cols_d, 128), cols_d)
 
     def e_at(g, f, t):
-        return e_all.at[:, pl.ds(pl.multiple_of(t * hid, 16), hid), cols_of(g, f)]
+        return e_all.at[g * n_fs + f, t]
 
     def s_at(g, f):
         return s_out.at[:, :, cols_of(g, f)]
@@ -181,12 +204,21 @@
 
     def turn(k, carry):
         here = pl.ds(pl.multiple_of(k * cols_d, 128), cols_d)
-        gate_out[here, :] = e_all[0, :, here].T
-        up_out[here, :] = e_all[1, :, here].T
+        gate_out[here, :] = e_all[k, :, 0].reshape(n_tp * hid, cols_d).T
+        up_out[here, :] = e_all[k, :, 1].reshape(n_tp * hid, cols_d).T
+        down_out[:, here] = e_all[k, :, 2].reshape(n_tp * hid, cols_d)
         s_gu[here, :] = s_out[0:2, :, here].reshape(2 * hid, cols_d).T
         return carry
 
     lax.fori_loop(0, n_gr * n_fs, turn, 0)
+    results = [
+        pltpu.make_async_copy(src, dst, res_sem.at[i])
+        for i, (src, dst) in enumerate((
+            (gate_out, gate_hbm), (up_out, up_hbm), (down_out, down_hbm),
+            (s_out.at[0], sg_hbm), (s_out.at[1], su_hbm), (s_out.at[2], sd_hbm),
+        ))
+    ]
+    start(results)
 
     step = 2
     chunk = min(width, 512)
@@ -221,7 +253,7 @@
 
             def cols(j, inner):
                 at = pl.ds(pl.multiple_of(j * chunk, 128), chunk)
-                res = jnp.dot(act, e_all[2, :, at], preferred_element_type=jnp.float32)
+                res = jnp.dot(act, down_out[:, at], preferred_element_type=jnp.float32)
                 res = res + jnp.dot(extra, s_out[2, :, at], preferred_element_type=jnp.float32)
                 part[pl.ds(first, step), :, :, at] = res.astype(jnp.bfloat16).reshape(
                     step, parts, sub, chunk
@@ -331,7 +363,8 @@
 
                     copy(t, h).start()
 
-    down_out[...] = e_all[2]
+    for one in results:
+        one.wait()
     for cond, copies in pending:
         if cond is None:
             for one in copies:
@@ -364,42 +397,34 @@
     plane, full, parts = n_fs * n_tp, n_gr * n_fs, 2
     sub = rows // parts
     bf16 = jnp.bfloat16
-    e_in = jnp.stack(
-        (
-            train_gate.transpose(0, 2, 1) * norm_gain,
-            train_up.transpose(0, 2, 1) * norm_gain,
-            train_down,
-        ),
-        axis=1,
-    ).astype(bf16)
-    s_in = jnp.stack(
-        (train_shared_gate.T * norm_gain, train_shared_up.T * norm_gain, train_shared_down)
-    ).astype(bf16)
-    widened = prompt.astype(jnp.float32)
-    normed = (
-        widened * lax.rsqrt(jnp.mean(widened * widened, axis=-1, keepdims=True) + eps_norm)
-    ).astype(bf16)
-    named = expert_ids.T[None, :, :] == jnp.arange(experts, dtype=jnp.int32)[:, None, None]
-    weights = jnp.sum(jnp.where(named, route_weight.T[None, :, :], 0.0), axis=1)
-
     vmem = pl.BlockSpec(memory_space=pltpu.VMEM)
     dma = pltpu.SemaphoreType.DMA
     shape = jax.ShapeDtypeStruct
-    serve_gate, serve_up, serve_down, s_all, mixed_out = pl.pallas_call(
+    serve_gate, serve_up, serve_down, s_gate, s_up, s_down, mixed_out = pl.pallas_call(
         functools.partial(plane_kernel, n_gr, n_fs, n_tp, parts),
         out_shape=(
             shape((width, n_tp * hid), bf16),
             shape((width, n_tp * hid), bf16),
             shape((n_tp * hid, width), bf16),
-            shape((3, hid, width), bf16),
+            shape((hid, width), bf16),
+            shape((hid, width), bf16),
+            shape((hid, width), bf16),
             shape((parts, sub, width), bf16),
         ),
-        in_specs=[vmem] * 4,
-        out_specs=(vmem,) * 5,
+        in_specs=[vmem] * 10,
+        out_specs=(pl.BlockSpec(memory_space=pl.ANY),) * 6 + (vmem,),
         scratch_shapes=[
+            pltpu.VMEM((parts, sub, width), bf16),
+            pltpu.VMEM((experts, rows), jnp.float32),
+            pltpu.VMEM((experts, 3, hid, rows_d), bf16),
+            pltpu.VMEM((3, hid, rows_d), bf16),
+            pltpu.VMEM((width, n_tp * hid), bf16),
+            pltpu.VMEM((width, n_tp * hid), bf16),
+            pltpu.VMEM((n_tp * hid, width), bf16),
+            pltpu.VMEM((3, hid, width), bf16),
             pltpu.VMEM((plane, parts, sub, width), bf16),
             pltpu.VMEM((plane, experts, rows), jnp.float32),
-            pltpu.VMEM((3, n_tp * hid, width), bf16),
+            pltpu.VMEM((full, n_tp, 3, hid, width // full), bf16),
             pltpu.VMEM((width, 2 * hid), bf16),
             pltpu.VMEM((plane, parts, sub, width), bf16),
             pltpu.VMEM((2, n_fs, parts, sub, width), bf16),
@@ -412,15 +437,19 @@
             dma((plane,)), dma((plane,)), dma((4 * n_fs,)), dma((4,)),
             dma((2,)), dma((2,)),
             dma((n_fs, parts)), dma((n_fs, parts)), dma((n_fs, parts)),
-            dma((n_fs, parts)), dma((n_fs, parts)), dma((n_fs, parts)),
+            dma((n_fs, parts)), dma((n_fs, parts)), dma((n_fs, parts)), dma((6,)),
         ],
         compiler_params=pltpu.CompilerParams(
             collective_id=0, has_side_effects=True, vmem_limit_bytes=VMEM_LIMIT
         ),
-    )(normed.reshape(parts, sub, width), weights, e_in, s_in)
+    )(
+        prompt, train_gate.transpose(0, 2, 1), train_up.transpose(0, 2, 1), train_down,
+        train_shared_gate.T, train_shared_up.T, train_shared_down, norm_gain[None, :],
+        expert_ids.T, route_weight.T,
+    )
     return (
         serve_gate[None], serve_up[None], serve_down[None],
-        s_all[0].T, s_all[1].T, s_all[2], mixed_out.reshape(rows, width),
+        s_gate.T, s_up.T, s_down, mixed_out.reshape(rows, width),
     )
 
 

time: 172 us -> 164 us (0.953)
  other arithmetic: 8.78 us -> 0 us
    another operation x6 -> x0, other arithmetic: 4 us -> none  [the longest x3 2.4 us: small_body(): jnp.stack((train_shared_gate.T * norm_gain, train_shared_up.T * norm_gain...]
    unnamed x20 -> x19, local copies, waits for them, and re-layouts: 4.79 us -> 8.29 us
    reduce_sum x2 -> x0, other arithmetic: 2.78 us -> none  [the longest x1 1.47 us: small_body(): weights = jnp.sum(jnp.where(named, route_weight.T[None, :, :], 0.0), axis=1)]
    squeeze x1 -> x0, local copies, waits for them, and re-layouts: 2.15 us -> none  [small_body(): s_all[2]]
    convert_element_type x1 -> x0, other arithmetic: 1.99 us -> none  [small_body(): normed = (widened * lax.rsqrt(jnp.mean(widened * widened, axis=-1, keepdi...]
where the time goes in v3:
time: 164 us; the launch traced here: 163 us
  Pallas kernels  154 us (94%)
  local copies, waits for them, and re-layouts  8.29 us (5%)
    pallas_call x1, Pallas kernels, small_body(): pl.pallas_call(functools.partial(plane_kernel, n_gr, n_fs, n_tp, parts),...  154 us
    unnamed x19, local copies, waits for them, and re-layouts  8.29 us

profile of v3, /device:TPU:24, one launch (start us, length us, event | category | flops | bytes accessed | tf_op | source)
XLA Modules:
  0.0 163.4 jit_solution(2169920224540976721)
XLA Ops:
  0.6 154.5 %shard_map.153 = (bf16[2048,256]{1,0:T(8,128)(2,1)}, bf16[2048,256]{1,0:T(8,128)(2,1)}, bf16[256,2048]{1,0:T(8,128)(2,1)}, bf16[64,2048]{1,0:T(8,128)(2,1)}, bf1...) custom-call(bf16[128,2048]{1,0:T(8,128)(2,1)} %p_ref.1, f32[16,64,256]{2,1,0:T(8,128)} %bitcast.16, ...), custom_call_target="tpu_custom_call" | custom-call | tf_op jit(solution)/shard_map/pallas_call | solution.py:403
  155.1 0.0 copy-start.1
  155.1 2.4 %copy.24 = bf16[1,2048,256]{2,1,0:T(8,128)(2,1)} copy(bf16[1,2048,256]{2,1,0:T(8,128)(2,1)} %bitcast.15) | data formatting | bytes 2097152
  157.5 0.0 copy-done.1
  157.5 0.0 copy-start
  157.5 1.0 copy.25
  158.4 0.6 copy-done
  159.1 0.0 copy-start.5
  159.1 1.0 copy.26
  160.0 0.1 copy-done.5
  160.2 0.0 copy-start.4
  160.2 0.0 copy-start.3
  160.2 0.7 copy.27
  160.9 0.3 copy-done.4
  161.2 0.0 copy-start.2
  161.2 0.7 copy.28
  161.9 0.0 copy-done.3
  161.9 0.7 copy.29
  162.6 0.0 copy-done.2
  162.6 0.8 copy.30
Async XLA Ops:
  155.1 2.4 %copy-start.1 = (bf16[2048,256]{1,0:T(8,128)(2,1)S(1)}, bf16[2048,256]{1,0:T(8,128)(2,1)}, u32[]{:S(2)}) copy-start(bf16[2048,256]{1,0:T(8,128)(2,1)} %get-tuple-element.15) | copy-start | bytes 3145732
  157.5 1.6 copy-start
  159.1 1.1 copy-start.5
  160.2 1.0 copy-start.4
  160.2 1.7 %copy-start.3 = (bf16[64,2048]{1,0:T(8,128)(2,1)S(1)}, bf16[64,2048]{1,0:T(8,128)(2,1)}, u32[]{:S(2)}) copy-start(bf16[64,2048]{1,0:T(8,128)(2,1)} %get-tuple-element.33) | copy-start | bytes 786436
  161.2 1.4 copy-start.2
